TPU v7x, 512 devices: a whole 4x4x16 slice. The times are simulated.
512 devices in a mesh: sp: 16 (over z), fs: 4 (over y), tp: 8 (over x, core).
Axes of the slice: x: 4, y: 4, z: 16, core: 2. Of those that a mesh axis runs over, the one named last changes fastest.
Arguments:
- tokens: bfloat16 [4, 16384, 2048], P('fs', 'sp', 'tp'), may hold values from -8 to 8
- norm_gain: float32 [2048], replicated, may hold values from 0.1 to 1.9
- w_query: bfloat16 [2048, 1024], P(('sp', 'fs'), 'tp'), may hold values from -4 to 4
- w_key: bfloat16 [2048, 512], P(('sp', 'fs'), 'tp'), may hold values from -0.16 to 0.16
- w_value: bfloat16 [2048, 512], P(('sp', 'fs'), 'tp'), may hold values from -0.125 to 0.125
- w_conv_in: bfloat16 [2048, 1024], P(('sp', 'fs'), 'tp'), may hold values from -0.125 to 0.125
- w_conv_b: bfloat16 [2048, 1024], P(('sp', 'fs'), 'tp'), may hold values from -0.125 to 0.125
- w_conv_c: bfloat16 [2048, 1024], P(('sp', 'fs'), 'tp'), may hold values from -0.125 to 0.125
- conv_taps: bfloat16 [3, 1024], P(None, 'tp'), may hold values from -3.5 to 3.5
- sink_logits: float32 [16], P('tp'), may hold values from 1 to 5
- w_attn_out: bfloat16 [1024, 2048], P('tp', ('sp', 'fs')), may hold values from -0.375 to 0.375
- w_conv_out: bfloat16 [1024, 2048], P('tp', ('sp', 'fs')), may hold values from -0.125 to 0.125
Outputs:
- mixed: bfloat16 [4, 16384, 2048], P('fs', ('sp', 'tp'))
All inputs are finite; a program needn't handle non-finite values.
Results may differ from a plain program's by a relative error of at most 0.02.
Values may be sent and summed in bfloat16 or wider, within the bound.
A program may use at most 128 MiB of HBM per device.

v0:
```python
import jax
import jax.numpy as jnp
from jax import lax
from jax.sharding import PartitionSpec as P

HEADS = 16
HEAD = 64
WINDOW = 128


def in_one_piece(arrays, axis, dim, along):
    widths = [a.shape[along] for a in arrays]
    both = jnp.concatenate(arrays, axis=along)
    whole = lax.all_gather(both, axis, axis=dim, tiled=True)
    return tuple(jnp.split(whole, [sum(widths[:k]) for k in range(1, len(widths))], axis=along))


def shifted(block, axis, distance):
    devices = range(lax.axis_size(axis))
    route = [(i - distance, i) for i in devices if i - distance in devices]
    return lax.ppermute(block, axis, route)


def rows_first(arrays, axis, dims):
    turned = [jnp.moveaxis(a, dim, 0) for a, dim in zip(arrays, dims)]
    both = jnp.concatenate([t.reshape(len(t), -1) for t in turned], axis=1)
    whole, at, finished = (lax.all_gather(both, axis, axis=0, tiled=True), 0, [])
    for t, dim in zip(turned, dims):
        share = whole[:, at : at + t[0].size].reshape(-1, *t.shape[1:])
        finished.append(jnp.moveaxis(share, 0, dim))
        at += t[0].size
    return tuple(finished)


def norm_rows(tokens, norm_gain):
    values = tokens.astype(jnp.float32)
    average = jnp.mean(values, axis=-1, keepdims=True)
    centred = values - average
    variance = jnp.mean(centred * centred, axis=-1, keepdims=True)
    return (centred * lax.rsqrt(variance + 1e-05) * norm_gain).astype(jnp.bfloat16)


def attend(queries, keys_values, earlier_rows, sink_logits, head_base, row_base):
    row_total = queries.shape[0]
    kv_cols = keys_values.shape[1] // 2
    kv_here = kv_cols // HEAD
    heads_here = queries.shape[1] // HEAD
    group = heads_here // kv_here
    keys_all = jnp.concatenate([earlier_rows, keys_values], axis=0)
    block_rows = min(512, row_total)
    head_ids = head_base + jnp.arange(heads_here, dtype=jnp.int32)
    slopes = jnp.exp2(-8.0 * (head_ids + 1).astype(jnp.float32) / HEADS).reshape(kv_here, group)[
        :, :, None, None
    ]
    sinks = sink_logits.reshape(kv_here, group)[:, :, None, None]
    row_ids = jnp.arange(block_rows, dtype=jnp.int32)[:, None]
    col_ids = jnp.arange(block_rows + WINDOW, dtype=jnp.int32)[None, :]
    distance = WINDOW + row_ids - col_ids
    outputs = []
    for block in range(row_total // block_rows):
        first_row = block * block_rows
        query_block = queries[first_row : first_row + block_rows].reshape(
            block_rows, kv_here, group, HEAD
        )
        band = keys_all[first_row : first_row + block_rows + WINDOW]
        band_keys = band[:, :kv_cols].reshape(block_rows + WINDOW, kv_here, HEAD)
        band_values = band[:, kv_cols:].reshape(block_rows + WINDOW, kv_here, HEAD)
        scores = jnp.einsum(
            "qkgd,skd->kgqs", query_block, band_keys, preferred_element_type=jnp.float32
        ) * HEAD ** (-0.5)
        scores = scores - slopes * distance.astype(jnp.float32)
        key_place = row_base + first_row - WINDOW + col_ids
        keep = (distance >= 0) & (distance < WINDOW) & (key_place >= 0)
        scores = jnp.where(keep, scores, -jnp.inf)
        highest = jnp.maximum(jnp.max(scores, axis=-1, keepdims=True), sinks)
        raised = jnp.exp(scores - highest)
        denominator = jnp.sum(raised, axis=-1, keepdims=True) + jnp.exp(sinks - highest)
        weights = (raised / denominator).astype(jnp.bfloat16)
        mixed = jnp.einsum(
            "kgqs,skd->qkgd", weights, band_values, preferred_element_type=jnp.float32
        )
        outputs.append(mixed.astype(jnp.bfloat16).reshape(block_rows, heads_here * HEAD))
    return jnp.concatenate(outputs, axis=0)


def on_device(
    tokens,
    norm_gain,
    w_query,
    w_key,
    w_value,
    w_conv_in,
    w_conv_b,
    w_conv_c,
    conv_taps,
    sink_logits,
    w_attn_out,
    w_conv_out,
):
    gathered = lax.all_gather(tokens, "tp", axis=2, tiled=True)[0]
    normed = norm_rows(gathered, norm_gain)
    row_total = normed.shape[0]
    weight_rows = in_one_piece(
        (w_query, w_key, w_value, w_conv_in, w_conv_b, w_conv_c), ("sp", "fs"), 0, 1
    )
    results = tuple(
        (
            jnp.dot(normed, rows_part, preferred_element_type=jnp.float32)
            for rows_part in weight_rows
        )
    )
    queries, keys, values, inner, gate_b, gate_c = tuple(
        (result.astype(jnp.bfloat16) for result in results)
    )
    product = (gate_c.astype(jnp.float32) * inner.astype(jnp.float32)).astype(jnp.bfloat16)
    keys_values = jnp.concatenate([keys, values], axis=1)
    earlier_kv, earlier_product = shifted(
        (keys_values[row_total - WINDOW :], product[row_total - 2 :]), "sp", 1
    )
    heads_here = queries.shape[1] // HEAD
    head_base = lax.axis_index("tp") * heads_here
    row_base = lax.axis_index("sp") * row_total
    attended = attend(queries, keys_values, earlier_kv, sink_logits, head_base, row_base)
    taps = conv_taps.astype(jnp.float32)
    padded = jnp.concatenate([earlier_product, product], axis=0).astype(jnp.float32)
    filtered = (
        taps[0] * padded[0:row_total]
        + taps[1] * padded[1 : row_total + 1]
        + taps[2] * padded[2 : row_total + 2]
    )
    conv_out = (gate_b.astype(jnp.float32) * filtered).astype(jnp.bfloat16)
    attn_columns, conv_columns = rows_first((w_attn_out, w_conv_out), ("sp", "fs"), (1, 1))
    summed = lax.psum_scatter(
        (
            jnp.dot(attended, attn_columns, preferred_element_type=jnp.float32)
            + jnp.dot(conv_out, conv_columns, preferred_element_type=jnp.float32)
        ).astype(jnp.bfloat16),
        "tp",
        scatter_dimension=0,
        tiled=True,
    )
    return summed[None]


def solution(mesh):
    placed = (
        P("fs", "sp", "tp"),
        P(),
        P(("sp", "fs"), "tp"),
        P(("sp", "fs"), "tp"),
        P(("sp", "fs"), "tp"),
        P(("sp", "fs"), "tp"),
        P(("sp", "fs"), "tp"),
        P(("sp", "fs"), "tp"),
        P(None, "tp"),
        P("tp"),
        P("tp", ("sp", "fs")),
        P("tp", ("sp", "fs")),
    )
    return jax.shard_map(
        on_device,
        mesh=mesh,
        in_specs=placed,
        out_specs=P("fs", ("sp", "tp"), None),
        check_vma=False,
    )
```

profile of v0, /device:TPU:8, one launch (start us, length us, event | category | flops | bytes accessed | tf_op | source)
XLA Modules:
  0.0 406.5 jit_solution(2349871307167087293)
XLA Ops:
  6.5 0.7 all-gather.4.cloned.1.call-update
  7.3 1.5 concatenate.18
  8.9 1.3 pad_maximum_fusion.4
  10.3 0.7 convert_element_type.108
  11.0 1.2 fusion.14
  12.2 0.5 fusion.32
  12.7 44.3 %all-gather.4.cloned.1.call-done = bf16[1,1024,2048]{2,1,0:T(8,128)(2,1)} async-done(((bf16[1,1024,256]{2,1,0:T(8,128)(2,1)}), bf16[1,1024,2048]{2,1,0:T(8,128)(2,1)}) %all-gather.4.cloned.1.call-update) | async-done | bytes 4194320 | tf_op jit(solution)/shard_map/all_gather | solution.py:100
  57.0 3.0 convert_reduce_fusion
  60.0 0.5 copy-done.1
  60.5 1.2 fusion.3
  61.7 3.0 fusion.5
  64.7 137.2 %all-gather.6.cloned.1.call-done = bf16[2048,640]{1,0:T(8,128)(2,1)} async-done(((bf16[32,640]{1,0:T(8,128)(2,1)}), bf16[2048,640]{1,0:T(8,128)(2,1)}) %all-gather.6.cloned.1.call-update) | async-done | bytes 2621456 | tf_op jit(solution)/shard_map/all_gather | solution.py:14
  201.9 3.9 convolution_convert_fusion.4
  205.8 2.6 convolution_convert_fusion.5
  208.4 3.7 collective-permute-start
  212.1 1.5 convolution_convert_fusion.3
  213.7 1.2 fusion.21
  214.9 1.3 fusion.20
  216.2 2.4 collective-permute-start.1
  218.7 0.9 fusion.65
  219.5 0.2 collective-permute-done.1
  219.8 0.9 fusion.64
  220.8 0.4 fusion.8
  221.1 0.1 exponential_add_fusion.1
  221.2 0.4 fusion.9
  221.6 0.1 exponential_add_fusion
  221.7 0.6 fusion.28
  222.3 0.6 fusion.25
  222.8 117.6 %all-gather.8.cloned.1.call-done = bf16[2048,256]{1,0:T(8,128)(2,1)} async-done(((bf16[32,256]{1,0:T(8,128)(2,1)}), bf16[2048,256]{1,0:T(8,128)(2,1)}) %all-gather.8.cloned.1.call-update) | async-done | bytes 1048592 | tf_op jit(solution)/shard_map/all_gather | solution.py:27
  340.4 5.6 %fusion.42 = f32[1024,2048]{1,0:T(8,128)} fusion(bf16[2048,256]{1,0:T(8,128)(2,1)} %all-gather.8.cloned.1.call-done, bf16[512,128]{0,1:T(8,128)(2,1)S(1)} %bitcast.77, bf16[512,128]{0,1:T(8,128)(2,1)S(1)} %bitcast.78), kind=kOutput, calls=%fused_computation.54 | convolution fusion | flops 537395200 | bytes 9175040 | tf_op jit(solution)/shard_map/dot_general | solution.py:135
  345.9 11.1 %add_convert_fusion = bf16[1024,2048]{1,0:T(8,128)(2,1)} fusion(f32[1024,2048]{1,0:T(8,128)} %fusion.42, bf16[1024,2048]{1,0:T(8,128)(2,1)} %fusion.5, bf16[2048,256]{1,0:T(8,128)(2,1)} %all-gather.8.cloned.1.call-done, f32[1026,128]{1,0:T(8,128)S(1)} %maximum_convert_fusion, bf16[2048,640]{1,0:T(8,128)(2,1)S(1)} %copy-done.2, f32[128]{0:T(128)S(1)} %get-tuple-element.8, ...), kind=kOutput, calls=%fused_computation.8 | convolution fusion | flops 1079115776 | bytes 19400192 | tf_op jit(solution)/shard_map/dot_general | solution.py:136
  357.1 42.9 %reduce-scatter.2.cloned.1.call-done = bf16[128,2048]{1,0:T(8,128)(2,1)} async-done(((bf16[1024,2048]{1,0:T(8,128)(2,1)}), bf16[128,2048]{1,0:T(8,128)(2,1)}) %reduce-scatter.2.cloned.1.call-update) | async-done | bytes 524304 | tf_op jit(solution)/shard_map/reduce_scatter | solution.py:133
  (30 shorter events, 0.4 us)
Async XLA Ops:
  6.5 50.5 %all-gather.4.cloned.1.call-start = ((), (), s32[]{:S(2)}) async-start(), calls=%async_computation.1 | async-start | bytes 4718592 | tf_op jit(solution)/shard_map/all_gather | solution.py:100
  7.3 194.6 %all-gather.6.cloned.1.call-start = ((), (), s32[]{:S(2)}) async-start(), calls=%async_computation.2 | async-start | bytes 2662400 | tf_op jit(solution)/shard_map/all_gather | solution.py:14
  8.8 331.6 %all-gather.8.cloned.1.call-start = ((), (), s32[]{:S(2)}) async-start(), calls=%async_computation.3 | async-start | bytes 1064960 | tf_op jit(solution)/shard_map/all_gather | solution.py:27
  10.2 389.8 %reduce-scatter.2.cloned.1.call-start = ((), (), s32[]{:S(2)}) async-start(), calls=%async_computation.4 | async-start | bytes 4718592 | tf_op jit(solution)/shard_map/reduce_scatter | solution.py:133
  57.0 3.4 copy-start.1
  60.0 1.7 copy-start.4
  201.9 3.9 copy-start
  205.8 6.3 %copy-start.2 = (bf16[2048,640]{1,0:T(8,128)(2,1)S(1)}, bf16[2048,640]{1,0:T(8,128)(2,1)}, u32[]{:S(2)}) copy-start(bf16[2048,640]{1,0:T(8,128)(2,1)} %all-gather.6.cloned.1.call-done) | copy-start | bytes 7864324
  208.4 11.4 %collective-permute-start = (bf16[128,128]{0,1:T(8,128)(2,1)S(1)}, bf16[128,128]{0,1:T(8,128)(2,1)S(1)}, u32[]{:S(2)}, u32[]{:S(2)}) collective-permute-start(bf16[128,128]{0,1:T(8,128)(2,1)S(1)} %pad_maximum_fusion.3), channel_id=1, source_target_pairs={{0,32},{32,64},{64,96},{96,128},{128,160},{160,192},{192,224},{224... | collective-permute-start | bytes 98312 | tf_op jit(solution)/shard_map/ppermute | solution.py:21
  214.9 3.7 copy-start.3
  216.2 3.5 collective-permute-start.1
  219.5 1.2 copy-start.5
Sparse Core Ops, SparseCore 0:
  9.4 47.5 all-gather.3
  60.0 141.8 all-gather.5
  204.8 135.5 all-gather.7
  357.2 42.6 reduce-scatter.1
where the time goes:
time: 407 us; the launch traced here: 406 us
  waiting for transfers between devices  343 us (84%)
  matrix products  30.1 us (7%)
  between operations  13.3 us (3%)
  other arithmetic  12 us (3%)
  starting transfers between devices  6.25 us (2%)
    all_gather x1, waiting for transfers between devices, in_one_piece(): whole = lax.all_gather(both, axis, axis=dim, tiled=True)  137 us
    all_gather x1, waiting for transfers between devices, rows_first(): lax.all_gather(both, axis, axis=0, tiled=True)  118 us
    all_gather x1, waiting for transfers between devices, on_device(): gathered = lax.all_gather(tokens, 'tp', axis=2, tiled=True)[0]  44.3 us
    reduce_scatter x1, waiting for transfers between devices, on_device(): lax.psum_scatter((jnp.dot(attended, attn_columns, preferred_element_type=...  42.9 us
    dot_general x1, matrix products, on_device(): jnp.dot(conv_out, conv_columns, preferred_element_type=jnp.float32)  11.1 us
    dot_general x5, matrix products, on_device(): jnp.dot(normed, rows_part, preferred_element_type=jnp.float32)  10.5 us
  transfers between devices with their start and end apart: 6, of which 5 were waited for; matrix products, arithmetic and copies ran while one was open for 7% of the time, Pallas kernels for 0%

commit v1 on v0

--- a/solution.py
+++ b/solution.py
@@ -6,6 +6,29 @@
 HEADS = 16
 HEAD = 64
 WINDOW = 128
+
+
+def take_roads_now(sheet, across):
+    o_now, next_value, local_part = (
+        lax.psum(1, axis_name=across),
+        lax.axis_index(across),
+        sheet.shape[2],
+    )
+    built, current_block = (sheet, 1)
+    while current_block < o_now:
+        built = jnp.concatenate(
+            [
+                built,
+                lax.ppermute(
+                    built,
+                    across,
+                    perm=tuple(((rr, (rr - current_block) % o_now) for rr in range(o_now))),
+                ),
+            ],
+            2,
+        )
+        current_block = 2 * current_block
+    return jnp.roll(built, next_value * local_part, axis=2)
 
 
 def in_one_piece(arrays, axis, dim, along):
@@ -97,7 +120,7 @@
     w_attn_out,
     w_conv_out,
 ):
-    gathered = lax.all_gather(tokens, "tp", axis=2, tiled=True)[0]
+    gathered = take_roads_now(tokens, across="tp")[0]
     normed = norm_rows(gathered, norm_gain)
     row_total = normed.shape[0]
     weight_rows = in_one_piece(

time: 407 us -> 360 us (0.88)
  waiting for transfers between devices: 343 us -> 286 us
  starting transfers between devices: 6.25 us -> 14.3 us
    all_gather x1, waiting for transfers between devices: 137 us -> 50.9 us  [in_one_piece(): whole = lax.all_gather(both, axis, axis=dim, tiled=True)]
    ppermute x0 -> x3, waiting for transfers between devices: none -> 74.2 us  [take_roads_now(): lax.ppermute(built, across, perm=tuple(((rr, (rr - current_block) % o_now...]
    all_gather x1 -> x0, waiting for transfers between devices: 44.3 us -> none  [on_device(): gathered = lax.all_gather(tokens, 'tp', axis=2, tiled=True)[0]]
    ppermute x0 -> x3, starting transfers between devices: none -> 7.97 us  [take_roads_now(): lax.ppermute(built, across, perm=tuple(((rr, (rr - current_block) % o_now...]
  transfers between devices with their start and end apart: 6 -> 8, of which waited for: 5 -> 6; matrix products, arithmetic and copies ran while one was open for 7% -> 8% of each run, Pallas kernels for 0% -> 0%
where the time goes in v1:
time: 360 us
  waiting for transfers between devices  286 us (79%)
  matrix products  30 us (8%)
  starting transfers between devices  14.3 us (4%)
  between operations  13.5 us (4%)
  other arithmetic  13 us (4%)
  local copies, waits for them, and re-layouts  3.68 us (1%)
    all_gather x1, waiting for transfers between devices, rows_first(): lax.all_gather(both, axis, axis=0, tiled=True)  118 us
    ppermute x3, waiting for transfers between devices, take_roads_now(): lax.ppermute(built, across, perm=tuple(((rr, (rr - current_block) % o_now...  74.2 us
    all_gather x1, waiting for transfers between devices, in_one_piece(): whole = lax.all_gather(both, axis, axis=dim, tiled=True)  50.9 us
    reduce_scatter x1, waiting for transfers between devices, on_device(): lax.psum_scatter((jnp.dot(attended, attn_columns, preferred_element_type=...  42.9 us
    dot_general x1, matrix products, on_device(): jnp.dot(conv_out, conv_columns, preferred_element_type=jnp.float32)  11.1 us
    dot_general x5, matrix products, on_device(): jnp.dot(normed, rows_part, preferred_element_type=jnp.float32)  10.5 us
    ppermute x3, starting transfers between devices, take_roads_now(): lax.ppermute(built, across, perm=tuple(((rr, (rr - current_block) % o_now...  7.97 us
  transfers between devices with their start and end apart: 8, of which 6 were waited for; matrix products, arithmetic and copies ran while one was open for 8% of the time, Pallas kernels for 0%

profile of v1, /device:TPU:8, one launch (start us, length us, event | category | flops | bytes accessed | tf_op | source)
XLA Modules:
  0.0 360.1 jit_solution(16152560940642645602)
XLA Ops:
  6.5 1.5 concatenate.35
  8.1 2.2 collective-permute-start
  10.3 7.0 %collective-permute-done = bf16[1,1024,256]{2,1,0:T(8,128)(2,1)S(1)} collective-permute-done((bf16[1,1024,256]{2,1,0:T(8,128)(2,1)}, bf16[1,1024,256]{2,1,0:T(8,128)(2,1)S(1)}, u32[]{:S(2)}, u32[]{:S(2)}) %collective-permute-start) | collective-permute-done | bytes 524320 | tf_op jit(solution)/shard_map/ppermute | solution.py:22
  17.3 1.3 pad_maximum_fusion.1
  18.7 2.9 collective-permute-start.1
  21.5 23.7 %collective-permute-done.1 = bf16[1,1024,512]{2,1,0:T(8,128)(2,1)S(1)} collective-permute-done((bf16[1,1024,512]{2,1,0:T(8,128)(2,1)S(1)}, bf16[1,1024,512]{2,1,0:T(8,128)(2,1)S(1)}, u32[]{:S(2)}, u32[]{:S(2)}) %collective-permute-start.1) | collective-permute-done | bytes 1048608 | tf_op jit(solution)/shard_map/ppermute | solution.py:22
  45.2 2.7 pad_maximum_fusion
  47.9 2.9 collective-permute-start.2
  50.8 0.6 pad_maximum_fusion.6
  51.6 1.1 constant_dynamic-update-slice_fusion.7
  52.8 1.2 fusion.32
  54.0 1.3 fusion.14
  55.5 43.5 %collective-permute-done.2 = bf16[1,1024,1024]{2,1,0:T(8,128)(2,1)S(1)} collective-permute-done((bf16[1,1024,1024]{2,1,0:T(8,128)(2,1)}, bf16[1,1024,1024]{2,1,0:T(8,128)(2,1)S(1)}, u32[]{:S(2)}, u32[]{:S(2)}) %collective-permute-start.2) | collective-permute-done | bytes 2097184 | tf_op jit(solution)/shard_map/ppermute | solution.py:22
  99.8 0.6 convert_reduce_fusion
  100.4 1.2 fusion.3
  101.7 3.0 fusion.5
  104.7 50.9 %all-gather.3.cloned.1.call-done = bf16[2048,640]{1,0:T(8,128)(2,1)} async-done(((bf16[32,640]{1,0:T(8,128)(2,1)}), bf16[2048,640]{1,0:T(8,128)(2,1)}) %all-gather.3.cloned.1.call-update) | async-done | bytes 2621456 | tf_op jit(solution)/shard_map/all_gather | solution.py:37
  155.6 3.7 %fusion.18 = f32[1024,128]{1,0:T(8,128)S(1)} fusion(bf16[1024,2048]{1,0:T(8,128)(2,1)} %fusion.5, bf16[2048,640]{1,0:T(8,128)(2,1)} %all-gather.3.cloned.1.call-done), kind=kOutput, calls=%fused_computation.30 | convolution fusion | flops 537133056 | bytes 5242880 | tf_op jit(solution)/shard_map/dot_general | solution.py:131
  159.3 2.4 fusion.21
  161.7 3.7 %collective-permute-start.4 = (bf16[2,128]{1,0:T(2,128)(2,1)S(1)}, bf16[2,128]{1,0:T(2,128)(2,1)S(1)}, u32[]{:S(2)}, u32[]{:S(2)}) collective-permute-start(bf16[2,128]{1,0:T(2,128)(2,1)S(1)} %slice.77), channel_id=1, source_target_pairs={{0,32},{32,64},{64,96},{96,128},{128,160},{160,192},{192,224},{224... | collective-permute-start | bytes 1544 | tf_op jit(solution)/shard_map/ppermute | solution.py:44
  165.4 1.5 convolution_convert_fusion.4
  166.9 1.4 convolution_convert_fusion.5
  168.3 2.5 collective-permute-start.3
  170.9 1.5 convolution_convert_fusion.3
  172.4 0.9 fusion.65
  173.4 0.9 fusion.64
  175.3 0.6 fusion.28
  175.9 0.6 fusion.25
  176.4 117.6 %all-gather.5.cloned.1.call-done = bf16[2048,256]{1,0:T(8,128)(2,1)} async-done(((bf16[32,256]{1,0:T(8,128)(2,1)}), bf16[2048,256]{1,0:T(8,128)(2,1)}) %all-gather.5.cloned.1.call-update) | async-done | bytes 1048592 | tf_op jit(solution)/shard_map/all_gather | solution.py:50
  294.0 5.5 %fusion.42 = f32[1024,2048]{1,0:T(8,128)} fusion(bf16[2048,256]{1,0:T(8,128)(2,1)} %all-gather.5.cloned.1.call-done, bf16[512,128]{0,1:T(8,128)(2,1)S(1)} %bitcast.77, bf16[512,128]{0,1:T(8,128)(2,1)S(1)} %bitcast.78), kind=kOutput, calls=%fused_computation.56 | convolution fusion | flops 537395200 | bytes 9175040 | tf_op jit(solution)/shard_map/dot_general | solution.py:158
  299.5 11.1 %add_convert_fusion = bf16[1024,2048]{1,0:T(8,128)(2,1)} fusion(f32[1024,2048]{1,0:T(8,128)} %fusion.42, bf16[1024,2048]{1,0:T(8,128)(2,1)} %fusion.5, bf16[2048,256]{1,0:T(8,128)(2,1)} %all-gather.5.cloned.1.call-done, f32[1026,128]{1,0:T(8,128)S(1)} %maximum_convert_fusion, bf16[2048,640]{1,0:T(8,128)(2,1)S(1)} %copy-done.4, f32[128]{0:T(128)S(1)} %get-tuple-element.8, ...), kind=kOutput, calls=%fused_computation.8 | convolution fusion | flops 1079115776 | bytes 19400192 | tf_op jit(solution)/shard_map/dot_general | solution.py:159
  310.7 42.9 %reduce-scatter.2.cloned.1.call-done = bf16[128,2048]{1,0:T(8,128)(2,1)} async-done(((bf16[1024,2048]{1,0:T(8,128)(2,1)}), bf16[128,2048]{1,0:T(8,128)(2,1)}) %reduce-scatter.2.cloned.1.call-update) | async-done | bytes 524304 | tf_op jit(solution)/shard_map/reduce_scatter | solution.py:156
  (55 shorter events, 2.3 us)
Async XLA Ops:
  6.5 149.0 %all-gather.3.cloned.1.call-start = ((), (), s32[]{:S(2)}) async-start(), calls=%async_computation.1 | async-start | bytes 2662400 | tf_op jit(solution)/shard_map/all_gather | solution.py:37
  8.0 286.0 %all-gather.5.cloned.1.call-start = ((), (), s32[]{:S(2)}) async-start(), calls=%async_computation.2 | async-start | bytes 1064960 | tf_op jit(solution)/shard_map/all_gather | solution.py:50
  8.1 9.2 %collective-permute-start = (bf16[1,1024,256]{2,1,0:T(8,128)(2,1)}, bf16[1,1024,256]{2,1,0:T(8,128)(2,1)S(1)}, u32[]{:S(2)}, u32[]{:S(2)}) collective-permute-start(bf16[1,1024,256]{2,1,0:T(8,128)(2,1)} %param.12), channel_id=1, source_target_pairs={{0,7},{1,0},{2,1},{3,2},{4,3},{5,4},{6,5},{7,6},{8,15},{9,8},{10,9... | collective-permute-start | bytes 1572872 | tf_op jit(solution)/shard_map/ppermute | solution.py:22
  17.3 30.6 %copy-start.2 = (bf16[1,1024,256]{2,1,0:T(8,128)(2,1)}, bf16[1,1024,256]{2,1,0:T(8,128)(2,1)S(1)}, u32[]{:S(2)}) copy-start(bf16[1,1024,256]{2,1,0:T(8,128)(2,1)S(1)} %collective-permute-done) | copy-start | bytes 1572868
  18.6 32.2 %copy-start.7 = (bf16[128,32]{0,1:T(8,128)(2,1)S(1)}, bf16[128,32]{0,1:T(8,128)(2,1)}, u32[]{:S(2)}) copy-start(bf16[128,32]{0,1:T(8,128)(2,1)} %param.23) | copy-start | bytes 24580
  18.6 32.2 %copy-start.8 = (bf16[128,32]{0,1:T(8,128)(2,1)S(1)}, bf16[128,32]{0,1:T(8,128)(2,1)}, u32[]{:S(2)}) copy-start(bf16[128,32]{0,1:T(8,128)(2,1)} %param.22) | copy-start | bytes 24580
  18.6 32.9 %copy-start.11 = (bf16[3,128]{1,0:T(4,128)(2,1)S(1)}, bf16[3,128]{1,0:T(4,128)(2,1)}, u32[]{:S(2)}) copy-start(bf16[3,128]{1,0:T(4,128)(2,1)} %param.20) | copy-start | bytes 2308
  18.7 26.6 %collective-permute-start.1 = (bf16[1,1024,512]{2,1,0:T(8,128)(2,1)S(1)}, bf16[1,1024,512]{2,1,0:T(8,128)(2,1)S(1)}, u32[]{:S(2)}, u32[]{:S(2)}) collective-permute-start(bf16[1,1024,512]{2,1,0:T(8,128)(2,1)S(1)} %pad_maximum_fusion.1), channel_id=1, source_target_pairs={{0,6},{1,7},{2,0},{3,1},{4,2},{5,3},{6,4},{7,5},{8,14},{9,15},{10,... | collective-permute-start | bytes 3145736 | tf_op jit(solution)/shard_map/ppermute | solution.py:22
  47.9 51.1 %collective-permute-start.2 = (bf16[1,1024,1024]{2,1,0:T(8,128)(2,1)}, bf16[1,1024,1024]{2,1,0:T(8,128)(2,1)S(1)}, u32[]{:S(2)}, u32[]{:S(2)}) collective-permute-start(bf16[1,1024,1024]{2,1,0:T(8,128)(2,1)} %pad_maximum_fusion), channel_id=1, source_target_pairs={{0,4},{1,5},{2,6},{3,7},{4,0},{5,1},{6,2},{7,3},{8,12},{9,13},{10,... | collective-permute-start | bytes 6291464 | tf_op jit(solution)/shard_map/ppermute | solution.py:22
  51.4 302.1 %reduce-scatter.2.cloned.1.call-start = ((), (), s32[]{:S(2)}) async-start(), calls=%async_computation.3 | async-start | bytes 4718592 | tf_op jit(solution)/shard_map/reduce_scatter | solution.py:156
  51.5 3.7 %copy-start.3 = (bf16[1,1024,256]{2,1,0:T(8,128)(2,1)S(1)}, bf16[1,1024,256]{2,1,0:T(8,128)(2,1)}, u32[]{:S(2)}) copy-start(bf16[1,1024,256]{2,1,0:T(8,128)(2,1)} %copy-done.2) | copy-start | bytes 1572868
  55.3 43.9 %copy-start.1 = (bf16[1,1024,256]{2,1,0:T(8,128)(2,1)S(1)}, bf16[1,1024,256]{2,1,0:T(8,128)(2,1)}, u32[]{:S(2)}) copy-start(bf16[1,1024,256]{2,1,0:T(8,128)(2,1)} %param.12) | copy-start | bytes 1572868
  100.4 1.3 copy-start.9
  155.6 3.7 %copy-start = (bf16[1024,2048]{1,0:T(8,128)(2,1)S(1)}, bf16[1024,2048]{1,0:T(8,128)(2,1)}, u32[]{:S(2)}) copy-start(bf16[1024,2048]{1,0:T(8,128)(2,1)} %fusion.5) | copy-start | bytes 12582916
  159.3 6.1 %copy-start.4 = (bf16[2048,640]{1,0:T(8,128)(2,1)S(1)}, bf16[2048,640]{1,0:T(8,128)(2,1)}, u32[]{:S(2)}) copy-start(bf16[2048,640]{1,0:T(8,128)(2,1)} %all-gather.3.cloned.1.call-done) | copy-start | bytes 7864324
  161.7 11.6 %collective-permute-start.4 = (bf16[2,128]{1,0:T(2,128)(2,1)S(1)}, bf16[2,128]{1,0:T(2,128)(2,1)S(1)}, u32[]{:S(2)}, u32[]{:S(2)}) collective-permute-start(bf16[2,128]{1,0:T(2,128)(2,1)S(1)} %slice.77), channel_id=1, source_target_pairs={{0,32},{32,64},{64,96},{96,128},{128,160},{160,192},{192,224},{224... | collective-permute-start | bytes 1544 | tf_op jit(solution)/shard_map/ppermute | solution.py:44
  168.3 4.1 %copy-start.5 = (f32[512,640]{0,1:T(8,128)S(1)}, f32[512,640]{0,1:T(8,128)}, u32[]{:S(2)}) copy-start(f32[512,640]{0,1:T(8,128)} %fusion.14) | copy-start | bytes 3932164
  168.3 4.1 %copy-start.6 = (pred[512,640]{0,1:T(8,128)(4,1)S(1)}, pred[512,640]{0,1:T(8,128)(4,1)}, u32[]{:S(2)}) copy-start(pred[512,640]{0,1:T(8,128)(4,1)} %get-tuple-element.11) | copy-start | bytes 983044
  168.3 5.1 %collective-permute-start.3 = (bf16[128,128]{0,1:T(8,128)(2,1)S(1)}, bf16[128,128]{0,1:T(8,128)(2,1)S(1)}, u32[]{:S(2)}, u32[]{:S(2)}) collective-permute-start(bf16[128,128]{0,1:T(8,128)(2,1)S(1)} %pad_maximum_fusion.5), channel_id=1, source_target_pairs={{0,32},{32,64},{64,96},{96,128},{128,160},{160,192},{192,224},{224... | collective-permute-start | bytes 98312 | tf_op jit(solution)/shard_map/ppermute | solution.py:44
  173.3 1.0 copy-start.10
Sparse Core Ops, SparseCore 0:
  10.3 145.2 all-gather.2
  158.5 135.4 all-gather.4
  310.8 42.6 reduce-scatter.1
